TPU v7x, 32 devices: a whole 2x2x4 slice. The times are simulated.
32 devices in a mesh: grp: 2 (over y), sp: 4 (over z), tp: 4 (over x, core).
Axes of the slice: x: 2, y: 2, z: 4, core: 2. Of those that a mesh axis runs over, the one named last changes fastest.
Arguments:
- latent: bfloat16 [3072, 4096], P(('grp', 'sp')), parts along dimension 0, may hold values from -6 to 6
- context: bfloat16 [512, 4096], P(('grp', 'sp')), parts along dimension 0, may hold values from -6 to 6
- cond_latent: bfloat16 [8192], P('grp'), parts along dimension 0, may hold values from -6 to 6
- cond_context: bfloat16 [4096], replicated, may hold values from -6 to 6
- w_shift: bfloat16 [4096, 4096], P('sp', 'tp'), may hold values from -0.09375 to 0.09375
- w_scale: bfloat16 [4096, 4096], P('sp', 'tp'), may hold values from -0.09375 to 0.09375
- w_gate: bfloat16 [4096, 4096], P('sp', 'tp'), may hold values from -0.1875 to 0.1875
- norm_gain: float32 [4096], replicated, may hold values from 0.1 to 1.9
- w_query: bfloat16 [4096, 2048], P(None, 'tp'), may hold values from -0.09375 to 0.09375
- w_key: bfloat16 [4096, 1024], P(None, 'tp'), may hold values from -0.09375 to 0.09375
- w_value: bfloat16 [4096, 1024], P(None, 'tp'), may hold values from -0.09375 to 0.09375
- q_gain: float32 [128], replicated, may hold values from 1 to 6.5, as said below
- k_gain: float32 [128], replicated, may hold values from 1 to 6.5, as said below
- w_out: bfloat16 [2048, 4096], P('tp'), may hold values from -0.5 to 0.5
Outputs:
- mixed: bfloat16 [3072, 4096], P(('grp', 'sp', 'tp')), parts along dimension 0
There are 2 independent parts, one for each index of `grp`. A program takes and returns all parts, laid end to end along the dimension named above; an argument that names none is the same for every part. Nothing has to cross between parts.
Inputs may be any that keep to these rules, and one draw needn't show every extreme that they name: `q_gain`: positive gains. `k_gain`: positive gains.
All inputs are finite; a program needn't handle non-finite values.
Results may differ from a plain program's by a relative error of at most 0.015.
The roundings to bfloat16 on the way count: a program that leaves them out, or rounds other values in their place, can miss the bound.
Values may be sent and summed in bfloat16 or wider, within the bound.
A program may use at most 128 MiB of HBM per device.

v0:
```python
import functools
import math

import jax
import jax.numpy as jnp
from jax import lax
from jax.experimental import pallas as pl
from jax.experimental.pallas import tpu as pltpu
from jax.sharding import PartitionSpec as P

HEADS = 16
KV_HEADS = 8
HEAD = 128
GRID_W = 64
GROUP = HEADS // KV_HEADS

epsilon = 1e-06
context_lift = 1.5
rope_theta = 10000.0

MESH = pl.DeviceIdType.MESH
f32 = jnp.float32
bf16 = jnp.bfloat16


def tile_of(rows, most):
    best = 16
    for size in range(16, most + 1, 16):
        if rows % size == 0:
            best = size
    return best


def kernel(
    n_sp,
    n_tp,
    tok,
    ctx,
    act_ref,
    gain_ref,
    q_gain_ref,
    k_gain_ref,
    latent_hbm,
    context_hbm,
    w_shift_hbm,
    w_scale_hbm,
    w_gate_hbm,
    w_query_hbm,
    w_key_hbm,
    w_value_hbm,
    w_out_hbm,
    out_ref,
    x,
    w_mod,
    w_query,
    w_key,
    w_value,
    w_out,
    inv,
    cos_ref,
    sin_a_ref,
    sin_b_ref,
    part,
    part_in,
    summed,
    mod,
    gate_part,
    gate_in,
    gate_sum,
    gate_mod,
    queries,
    kv,
    top,
    total,
    acc,
    attended,
    pair_out,
    pair_in,
    mine,
    far_out,
    far_in,
    load_sem,
    mod_send,
    mod_recv,
    mod2_send,
    mod2_recv,
    gate_send,
    gate_recv,
    gate2_send,
    gate2_recv,
    right_send,
    right_recv,
    left_send,
    left_recv,
    pair_send,
    pair_recv,
    far_send,
    far_recv,
):
    sp = lax.axis_index("sp")
    tp = lax.axis_index("tp")
    rows = tok + ctx
    depth = x.shape[1]
    mod_cols = mod.shape[2]
    heads = queries.shape[1] // HEAD
    kv_cols = kv.shape[2] // 2
    kv_heads = kv_cols // HEAD
    kv_tile = tile_of(rows, 128)
    kv_chunks = rows // kv_tile
    per_unit = 2 if kv_chunks % 2 == 0 else 1
    units = kv_chunks // per_unit
    unit_rows = kv_tile * per_unit

    loads = {}

    def load(name, index, source, target):
        loads[name] = pltpu.make_async_copy(source, target, load_sem.at[index])
        loads[name].start()

    load("shift", 0, w_shift_hbm, w_mod.at[0])
    load("scale", 1, w_scale_hbm, w_mod.at[1])
    load("latent", 3, latent_hbm, x.at[pl.ds(0, tok)])
    load("context", 4, context_hbm, x.at[pl.ds(tok, ctx)])

    barrier = pltpu.get_barrier_semaphore()
    for k in range(1, n_sp):
        pl.semaphore_signal(
            barrier, inc=1, device_id={"sp": lax.rem(sp + k, n_sp)}, device_id_type=MESH
        )
    for k in range(1, n_tp):
        pl.semaphore_signal(
            barrier, inc=1, device_id={"tp": lax.rem(tp + k, n_tp)}, device_id_type=MESH
        )

    act = act_ref[...]
    for which, name in enumerate(("shift", "scale")):
        loads[name].wait()
        got = jnp.dot(act, w_mod[which], preferred_element_type=f32)
        part[2 * which : 2 * which + 2, :] = got[0:2, :]
    pl.semaphore_wait(barrier, n_sp + n_tp - 2)

    def mod_copy(k):
        return pltpu.make_async_remote_copy(
            src_ref=part,
            dst_ref=part_in.at[k - 1],
            send_sem=mod_send.at[k - 1],
            recv_sem=mod_recv.at[k - 1],
            device_id={"sp": lax.rem(sp + k, n_sp)},
            device_id_type=MESH,
        )

    for k in range(1, n_sp):
        mod_copy(k).start()
    load("gate", 2, w_gate_hbm, w_mod.at[2])
    load("key", 5, w_key_hbm, w_key)
    load("value", 6, w_value_hbm, w_value)
    load("query", 7, w_query_hbm, w_query)
    load("out", 8, w_out_hbm, w_out)

    def tables(i, carry):
        at = pl.ds(pl.multiple_of(i * 16, 16), 16)
        index = i * 16 + lax.broadcasted_iota(jnp.int32, (16, HEAD), 0)
        lane = lax.broadcasted_iota(jnp.int32, (16, HEAD), 1)
        freqs = HEAD // 4
        position = sp * tok + index
        inverse = jnp.exp(lax.rem(lane, freqs).astype(f32) * (-math.log(rope_theta) / freqs))
        place = jnp.where(lane < 2 * freqs, lax.div(position, GRID_W), lax.rem(position, GRID_W))
        angle = jnp.where(index < tok, place.astype(f32) * inverse, 0.0)
        sine = jnp.sin(angle)
        first_half = lax.rem(lax.div(lane, freqs), 2) == 0
        cos_ref[at, :] = jnp.cos(angle)
        sin_a_ref[at, :] = jnp.where(first_half, -sine, 0.0)
        sin_b_ref[at, :] = jnp.where(first_half, 0.0, sine)
        return carry

    lax.fori_loop(0, rows // 16, tables, 0)
    loads["latent"].wait()
    loads["context"].wait()

    def stats(i, carry):
        at = pl.ds(pl.multiple_of(i * 16, 16), 16)
        piece = x[at, :].astype(f32)
        inv[at, :] = lax.rsqrt(jnp.mean(piece * piece, axis=-1, keepdims=True) + epsilon)
        return carry

    lax.fori_loop(0, rows // 16, stats, 0, unroll=2)

    for k in range(1, n_sp):
        mod_copy(k).wait_recv()
    whole = part[...]
    for k in range(1, n_sp):
        whole = whole + part_in[k - 1]
    summed[...] = whole
    mod[tp] = whole

    def mod2_copy(k):
        return pltpu.make_async_remote_copy(
            src_ref=summed,
            dst_ref=mod.at[tp],
            send_sem=mod2_send.at[k - 1],
            recv_sem=mod2_recv.at[k - 1],
            device_id={"tp": lax.rem(tp + k, n_tp)},
            device_id_type=MESH,
        )

    for k in range(1, n_tp):
        mod2_copy(k).start()

    def gate_copy(k):
        return pltpu.make_async_remote_copy(
            src_ref=gate_part,
            dst_ref=gate_in.at[k - 1],
            send_sem=gate_send.at[k - 1],
            recv_sem=gate_recv.at[k - 1],
            device_id={"sp": lax.rem(sp + k, n_sp)},
            device_id_type=MESH,
        )

    def gate2_copy(k):
        return pltpu.make_async_remote_copy(
            src_ref=gate_sum,
            dst_ref=gate_mod.at[tp],
            send_sem=gate2_send.at[k - 1],
            recv_sem=gate2_recv.at[k - 1],
            device_id={"tp": lax.rem(tp + k, n_tp)},
            device_id_type=MESH,
        )

    loads["gate"].wait()
    gate_part[...] = jnp.dot(act, w_mod[2], preferred_element_type=f32)[0:2, :]
    for k in range(1, n_sp):
        gate_copy(k).start()
    for k in range(1, n_tp):
        mod2_copy(k).wait_recv()

    def normalize(low, high):
        for start in range(low, high, 16):
            row = 0 if start < tok else 1
            at = slice(start, start + 16)
            for j in range(n_tp):
                cols = slice(j * mod_cols, (j + 1) * mod_cols)
                factor = gain_ref[:, cols] * (1.0 + mod[j, 2 + row : 3 + row, :])
                shift = mod[j, row : row + 1, :]
                piece = x[at, cols].astype(f32)
                x[at, cols] = (piece * inv[at, :] * factor + shift).astype(bf16)

    def turn(vector, gain, at):
        vector = vector * lax.rsqrt(jnp.mean(vector * vector, axis=-1, keepdims=True) + epsilon) * gain
        ahead = pltpu.roll(vector, HEAD - HEAD // 4, 1)
        behind = pltpu.roll(vector, HEAD // 4, 1)
        return vector * cos_ref[at, :] + ahead * sin_a_ref[at, :] + behind * sin_b_ref[at, :]

    def stream_copy(block, step, c, send, recv, to):
        held = kv.at[block, pl.ds(pl.multiple_of(c * kv_tile, 16), kv_tile)]
        return pltpu.make_async_remote_copy(
            src_ref=held,
            dst_ref=held,
            send_sem=send.at[step, c],
            recv_sem=recv.at[step, c],
            device_id={"sp": to},
            device_id_type=MESH,
        )

    to_right = jnp.minimum(sp + 1, n_sp - 1)
    to_left = jnp.maximum(sp - 1, 0)

    def right_copy(step, c):
        return stream_copy(jnp.maximum(sp - step, 0), step, c, right_send, right_recv, to_right)

    def left_copy(step, c):
        return stream_copy(jnp.minimum(sp + step, n_sp - 1), step, c, left_send, left_recv, to_left)

    def right_arrival(step, c):
        return stream_copy(jnp.maximum(sp - 1 - step, 0), step, c, right_send, right_recv, to_right)

    def left_arrival(step, c):
        return stream_copy(
            jnp.minimum(sp + 1 + step, n_sp - 1), step, c, left_send, left_recv, to_left
        )

    for c in range(kv_chunks):
        low, high = c * kv_tile, (c + 1) * kv_tile
        at = slice(low, high)
        normalize(low, high)
        if c == 0:
            loads["key"].wait()
            loads["value"].wait()
        raw = jnp.dot(x[at, :], w_key[...], preferred_element_type=f32)
        raw_values = jnp.dot(x[at, :], w_value[...], preferred_element_type=f32)
        for h in range(kv_heads):
            cols = slice(h * HEAD, (h + 1) * HEAD)
            kv[sp, at, cols] = turn(raw[:, cols], k_gain_ref[...], at).astype(bf16)
        kv[sp, at, kv_cols:] = raw_values.astype(bf16)

        @pl.when(sp < n_sp - 1)
        def _():
            right_copy(0, c).start()

        @pl.when(sp > 0)
        def _():
            left_copy(0, c).start()

    q_tile = tile_of(tok, 256)

    def project_queries(i, carry):
        at = pl.ds(pl.multiple_of(i * q_tile, 16), q_tile)
        raw = jnp.dot(x[at, :], w_query[...], preferred_element_type=f32)
        for h in range(heads):
            cols = slice(h * HEAD, (h + 1) * HEAD)
            queries[at, cols] = turn(raw[:, cols], q_gain_ref[...], at).astype(bf16)
        return carry

    loads["query"].wait()
    lax.fori_loop(0, tok // q_tile, project_queries, 0)

    scaling = HEAD ** (-0.5)
    a_tile = tile_of(tok, 128)

    def attend(block, unit, first):
        held = pl.ds(pl.multiple_of(unit * unit_rows, 16), unit_rows)
        lane = unit * unit_rows + lax.broadcasted_iota(jnp.int32, (1, unit_rows), 1)
        lift = jnp.where(lane >= tok, context_lift, 0.0).astype(f32)
        spans = [slice(h * HEAD, (h + 1) * HEAD) for h in range(heads)]

        def one(i, carry):
            at = pl.ds(pl.multiple_of(i * a_tile, 16), a_tile)
            scores = []
            for h in range(heads):
                kv_span = slice((h // GROUP) * HEAD, (h // GROUP + 1) * HEAD)
                scores.append(
                    lax.dot_general(
                        queries[at, spans[h]],
                        kv[block, held, kv_span],
                        (((1,), (1,)), ((), ())),
                        preferred_element_type=f32,
                    )
                    * scaling
                    + lift
                )
            highs, fades, sums, products = [], [], [], []
            for h in range(heads):
                high = jnp.max(scores[h], axis=-1, keepdims=True)
                if not first:
                    old = top[h, at, :]
                    high = jnp.maximum(high, old)
                    fades.append(jnp.exp(old - high))
                highs.append(high)
                weights = jnp.exp(scores[h] - high)
                sums.append(jnp.sum(weights, axis=-1, keepdims=True))
                begin = kv_cols + (h // GROUP) * HEAD
                products.append(
                    jnp.dot(
                        weights.astype(bf16),
                        kv[block, held, begin : begin + HEAD],
                        preferred_element_type=f32,
                    )
                )
            if not first:
                sums = [total[h, at, :] * fades[h] + sums[h] for h in range(heads)]
                products = [acc[at, spans[h]] * fades[h] + products[h] for h in range(heads)]
            for h in range(heads):
                top[h, at, :] = highs[h]
                total[h, at, :] = sums[h]
                acc[at, spans[h]] = products[h]
            return carry

        lax.fori_loop(0, tok // a_tile, one, 0)

    attend(sp, 0, True)
    for unit in range(1, units):
        attend(sp, unit, False)

    for k in range(1, n_sp):
        gate_copy(k).wait_recv()
    gate_whole = gate_part[...]
    for k in range(1, n_sp):
        gate_whole = gate_whole + gate_in[k - 1]
    gate_sum[...] = gate_whole
    gate_mod[tp] = gate_whole
    for k in range(1, n_tp):
        gate2_copy(k).start()

    def gather_step(t, carry):
        step = t // units
        unit = lax.rem(t, units)
        from_left = sp - 1 - step >= 0
        from_right = sp + 1 + step <= n_sp - 1
        for k in range(per_unit):
            c = unit * per_unit + k

            @pl.when(from_left)
            def _():
                right_arrival(step, c).wait_recv()

                @pl.when(sp < n_sp - 1)
                def _():
                    right_copy(step + 1, c).start()

            @pl.when(from_right)
            def _():
                left_arrival(step, c).wait_recv()

                @pl.when(sp > 0)
                def _():
                    left_copy(step + 1, c).start()

        @pl.when(from_left)
        def _():
            attend(jnp.maximum(sp - 1 - step, 0), unit, False)

        @pl.when(from_right)
        def _():
            attend(jnp.minimum(sp + 1 + step, n_sp - 1), unit, False)

        return carry

    lax.fori_loop(0, (n_sp - 1) * units, gather_step, 0)

    def finish(i, carry):
        at = pl.ds(pl.multiple_of(i * a_tile, 16), a_tile)
        for h in range(heads):
            cols = slice(h * HEAD, (h + 1) * HEAD)
            attended[at, cols] = (acc[at, cols] / total[h, at, :]).astype(bf16)
        return carry

    lax.fori_loop(0, tok // a_tile, finish, 0)

    chips = n_tp // 2
    chip = tp // 2
    core = lax.rem(tp, 2)
    piece = tok // n_tp
    width = pair_out.shape[3]
    chunks = depth // width

    def pair_copy(k, c):
        return pltpu.make_async_remote_copy(
            src_ref=pair_out.at[k, c],
            dst_ref=pair_in.at[k, c],
            send_sem=pair_send.at[k, c],
            recv_sem=pair_recv.at[k, c],
            device_id={"tp": chip * 2 + 1 - core},
            device_id_type=MESH,
        )

    def far_copy(k, c):
        return pltpu.make_async_remote_copy(
            src_ref=far_out.at[k - 1, c],
            dst_ref=far_in.at[k - 1, c],
            send_sem=far_send.at[k - 1, c],
            recv_sem=far_recv.at[k - 1, c],
            device_id={"tp": lax.rem(chip + k, chips) * 2 + core},
            device_id_type=MESH,
        )

    def multiply(k, c):
        to = lax.rem(chip + k, chips)
        cols = pl.ds(pl.multiple_of(c * width, width), width)

        def part_of(which):
            at = pl.ds(pl.multiple_of((to * 2 + which) * piece, 16), piece)
            return jnp.dot(
                attended[at, :], w_out[:, cols], preferred_element_type=f32
            ).astype(bf16)

        pair_out[k, c] = part_of(1 - core)
        pair_copy(k, c).start()
        mine[k, c] = part_of(core)

    def combine(k, c):
        pair_copy(k, c).wait_recv()
        far_out[k - 1, c] = (mine[k, c].astype(f32) + pair_in[k, c].astype(f32)).astype(bf16)
        far_copy(k, c).start()

    loads["out"].wait()
    for k in range(1, chips):
        multiply(k, 0)

        def far_step(c, carry):
            multiply(k, c)
            combine(k, c - 1)
            return carry

        lax.fori_loop(1, chunks, far_step, 0)
        combine(k, chunks - 1)

    def near_step(c, carry):
        multiply(0, c)
        return carry

    lax.fori_loop(0, chunks, near_step, 0)

    for k in range(1, n_tp):
        gate2_copy(k).wait_recv()
    per = mod_cols // width
    for c in range(chunks):
        pair_copy(0, c).wait_recv()
        result = mine[0, c].astype(f32) + pair_in[0, c].astype(f32)
        for k in range(1, chips):
            far_copy(k, c).wait_recv()
            result = result + far_in[k - 1, c].astype(f32)
        first = (c % per) * width
        gate = gate_mod[c // per, 0:1, first : first + width]
        out_ref[:, c * width : (c + 1) * width] = (gate * result).astype(bf16)

    for k in range(1, n_sp):
        mod_copy(k).wait_send()
        gate_copy(k).wait_send()
    for k in range(1, n_tp):
        mod2_copy(k).wait_send()
        gate2_copy(k).wait_send()

    def drain(step, carry):
        for which in range(kv_chunks):

            @pl.when(jnp.logical_and(sp < n_sp - 1, sp - step >= 0))
            def _():
                right_copy(step, which).wait_send()

            @pl.when(jnp.logical_and(sp > 0, sp + step <= n_sp - 1))
            def _():
                left_copy(step, which).wait_send()

        return carry

    lax.fori_loop(0, n_sp - 1, drain, 0)
    for c in range(chunks):
        pair_copy(0, c).wait_send()
        for k in range(1, chips):
            pair_copy(k, c).wait_send()
            far_copy(k, c).wait_send()


def body(
    n_sp,
    n_tp,
    latent,
    context,
    cond_latent,
    cond_context,
    w_shift,
    w_scale,
    w_gate,
    norm_gain,
    w_query,
    w_key,
    w_value,
    q_gain,
    k_gain,
    w_out,
):
    sp = lax.axis_index("sp")
    tok, depth = latent.shape
    ctx = context.shape[0]
    rows = tok + ctx
    mod_rows, mod_cols = w_shift.shape
    mine = [
        lax.dynamic_slice_in_dim(cond, sp * mod_rows, mod_rows, 0)
        for cond in (cond_latent, cond_context)
    ]
    row = lax.broadcasted_iota(jnp.int32, (16, mod_rows), 0)
    act = jnp.where(row == 0, mine[0][None].astype(f32), mine[1][None].astype(f32))
    act = jnp.where(row < 2, jax.nn.silu(act), 0.0).astype(bf16)
    chips = n_tp // 2
    piece = tok // n_tp
    width = min(512, mod_cols)
    chunks = depth // width
    kv_cols = w_key.shape[1]
    q_cols = w_query.shape[1]
    heads = q_cols // HEAD
    vmem = pl.BlockSpec(memory_space=pltpu.VMEM)
    hbm = pl.BlockSpec(memory_space=pl.ANY)
    dma = pltpu.SemaphoreType.DMA
    far = max(chips - 1, 1)
    kv_chunks = rows // tile_of(rows, 128)
    return pl.pallas_call(
        functools.partial(kernel, n_sp, n_tp, tok, ctx),
        out_shape=jax.ShapeDtypeStruct((piece, depth), bf16),
        in_specs=[vmem] * 4 + [hbm] * 9,
        out_specs=vmem,
        scratch_shapes=[
            pltpu.VMEM((rows, depth), bf16),
            pltpu.VMEM((3, mod_rows, mod_cols), bf16),
            pltpu.VMEM(w_query.shape, bf16),
            pltpu.VMEM(w_key.shape, bf16),
            pltpu.VMEM(w_value.shape, bf16),
            pltpu.VMEM(w_out.shape, bf16),
            pltpu.VMEM((rows, 1), f32),
            pltpu.VMEM((rows, HEAD), f32),
            pltpu.VMEM((rows, HEAD), f32),
            pltpu.VMEM((rows, HEAD), f32),
            pltpu.VMEM((4, mod_cols), f32),
            pltpu.VMEM((n_sp - 1, 4, mod_cols), f32),
            pltpu.VMEM((4, mod_cols), f32),
            pltpu.VMEM((n_tp, 4, mod_cols), f32),
            pltpu.VMEM((2, mod_cols), f32),
            pltpu.VMEM((n_sp - 1, 2, mod_cols), f32),
            pltpu.VMEM((2, mod_cols), f32),
            pltpu.VMEM((n_tp, 2, mod_cols), f32),
            pltpu.VMEM((tok, q_cols), bf16),
            pltpu.VMEM((n_sp, rows, 2 * kv_cols), bf16),
            pltpu.VMEM((heads, tok, 1), f32),
            pltpu.VMEM((heads, tok, 1), f32),
            pltpu.VMEM((tok, q_cols), f32),
            pltpu.VMEM((tok, q_cols), bf16),
            pltpu.VMEM((chips, chunks, piece, width), bf16),
            pltpu.VMEM((chips, chunks, piece, width), bf16),
            pltpu.VMEM((chips, chunks, piece, width), bf16),
            pltpu.VMEM((far, chunks, piece, width), bf16),
            pltpu.VMEM((far, chunks, piece, width), bf16),
            dma((9,)),
            dma((n_sp - 1,)),
            dma((n_sp - 1,)),
            dma((n_tp - 1,)),
            dma((n_tp - 1,)),
            dma((n_sp - 1,)),
            dma((n_sp - 1,)),
            dma((n_tp - 1,)),
            dma((n_tp - 1,)),
            dma((n_sp, kv_chunks)),
            dma((n_sp, kv_chunks)),
            dma((n_sp, kv_chunks)),
            dma((n_sp, kv_chunks)),
            dma((chips, chunks)),
            dma((chips, chunks)),
            dma((far, chunks)),
            dma((far, chunks)),
        ],
        compiler_params=pltpu.CompilerParams(
            collective_id=0, has_side_effects=True, vmem_limit_bytes=60 * 1024 * 1024
        ),
    )(
        act,
        norm_gain.reshape(1, depth),
        q_gain.reshape(1, HEAD),
        k_gain.reshape(1, HEAD),
        latent,
        context,
        w_shift,
        w_scale,
        w_gate,
        w_query,
        w_key,
        w_value,
        w_out,
    )


def solution(mesh):
    placed = (
        P(("grp", "sp"), None),
        P(("grp", "sp"), None),
        P("grp"),
        P(),
        P("sp", "tp"),
        P("sp", "tp"),
        P("sp", "tp"),
        P(),
        P(None, "tp"),
        P(None, "tp"),
        P(None, "tp"),
        P(),
        P(),
        P("tp", None),
    )
    return jax.shard_map(
        functools.partial(body, mesh.shape["sp"], mesh.shape["tp"]),
        mesh=mesh,
        in_specs=placed,
        out_specs=P(("grp", "sp", "tp"), None),
        check_vma=False,
    )
```

profile of v0, /device:TPU:0, one launch (start us, length us, event | category | flops | bytes accessed | tf_op | source)
XLA Modules:
  0.0 75.3 jit_solution(7113962984685423807)
XLA Ops:
  0.0 0.7 dynamic-slice_convert_fusion
  0.7 0.7 fusion.4.act_ref
  1.4 71.8 %shard_map.136 = bf16[96,4096]{1,0:T(8,128)(2,1)} custom-call(bf16[16,1024]{1,0:T(8,128)(2,1)} %fusion.4.act_ref, f32[1,4096]{1,0:T(1,128)} %bitcast.3, f32[1,128]{1,0:T(1,128)} %bitcast.4, f32[1,128]{1,0:T(1,128)} %bitcast.5, bf16[384,4096]{1,0:T(8,128)(2,1)} %latent_hbm.1, bf16[64,4096]{1,0:T(8,128)(2,1)} %context_hbm.1, bf16[1024,1024]{1,0:T(8,128)(2,1)} %w_shift_hbm.1, ...), custom_call_target="tpu_custom_call" | custom-call | tf_op jit(solution)/shard_map/pallas_call | solution.py:575
  73.2 2.1 %copy.16 = bf16[96,4096]{1,0:T(8,128)(2,1)} copy(bf16[96,4096]{1,0:T(8,128)(2,1)} %shard_map.136) | data formatting | bytes 1572864
  (1 shorter events, 0.0 us)
where the time goes:
time: 75.5 us; the launch traced here: 75.3 us
  Pallas kernels  71.8 us (95%)
  local copies, waits for them, and re-layouts  2.06 us (3%)
  other arithmetic  1.42 us (2%)
    pallas_call x1, Pallas kernels, body(): pl.pallas_call(functools.partial(kernel, n_sp, n_tp, tok, ctx), out_shape...  71.8 us
    unnamed x1, local copies, waits for them, and re-layouts  2.06 us

commit v1 on v0

--- a/solution.py
+++ b/solution.py
@@ -32,11 +32,14 @@
 
 
 def kernel(
+    n_grp,
     n_sp,
     n_tp,
     tok,
     ctx,
-    act_ref,
+    share,
+    cond_latent_ref,
+    cond_context_ref,
     gain_ref,
     q_gain_ref,
     k_gain_ref,
@@ -50,12 +53,14 @@
     w_value_hbm,
     w_out_hbm,
     out_ref,
+    act_ref,
     x,
     w_mod,
     w_query,
     w_key,
     w_value,
-    w_out,
+    w_all,
+    w_rest,
     inv,
     cos_ref,
     sin_a_ref,
@@ -74,6 +79,8 @@
     total,
     acc,
     attended,
+    att_all,
+    acc_out,
     pair_out,
     pair_in,
     mine,
@@ -96,9 +103,29 @@
     pair_recv,
     far_send,
     far_recv,
+    own_send,
+    own_recv,
+    across_send,
+    across_recv,
+    beside_send,
+    beside_recv,
+    over_send,
+    over_recv,
+    last_send,
+    last_recv,
+    att_send,
+    att_recv,
 ):
+    grp = lax.axis_index("grp")
     sp = lax.axis_index("sp")
     tp = lax.axis_index("tp")
+    chips = n_tp // 2
+    chip = tp // 2
+    core = lax.rem(tp, 2)
+    partner = chip * 2 + 1 - core
+    piece = tok // n_tp
+    turns = w_all.shape[2] // (n_grp * share)
+    shared = w_all.shape[2]
     rows = tok + ctx
     depth = x.shape[1]
     mod_cols = mod.shape[2]
@@ -132,30 +159,10 @@
             barrier, inc=1, device_id={"tp": lax.rem(tp + k, n_tp)}, device_id_type=MESH
         )
 
-    act = act_ref[...]
-    for which, name in enumerate(("shift", "scale")):
-        loads[name].wait()
-        got = jnp.dot(act, w_mod[which], preferred_element_type=f32)
-        part[2 * which : 2 * which + 2, :] = got[0:2, :]
-    pl.semaphore_wait(barrier, n_sp + n_tp - 2)
-
-    def mod_copy(k):
-        return pltpu.make_async_remote_copy(
-            src_ref=part,
-            dst_ref=part_in.at[k - 1],
-            send_sem=mod_send.at[k - 1],
-            recv_sem=mod_recv.at[k - 1],
-            device_id={"sp": lax.rem(sp + k, n_sp)},
-            device_id_type=MESH,
-        )
-
-    for k in range(1, n_sp):
-        mod_copy(k).start()
-    load("gate", 2, w_gate_hbm, w_mod.at[2])
-    load("key", 5, w_key_hbm, w_key)
-    load("value", 6, w_value_hbm, w_value)
-    load("query", 7, w_query_hbm, w_query)
-    load("out", 8, w_out_hbm, w_out)
+    for k in range(1, n_grp):
+        pl.semaphore_signal(
+            barrier, inc=1, device_id={"grp": lax.rem(grp + k, n_grp)}, device_id_type=MESH
+        )
 
     def tables(i, carry):
         at = pl.ds(pl.multiple_of(i * 16, 16), 16)
@@ -174,6 +181,121 @@
         return carry
 
     lax.fori_loop(0, rows // 16, tables, 0)
+    mod_rows = w_mod.shape[1]
+    vectors = [ref[...].astype(f32) for ref in (cond_latent_ref, cond_context_ref)]
+    vectors = [vector * (1.0 / (1.0 + jnp.exp(-vector))) for vector in vectors]
+    lane_rows = depth // HEAD
+    for j in range(lane_rows):
+        pair = [vector[j : j + 1, :] for vector in vectors]
+        act_ref[0:2, j * HEAD : (j + 1) * HEAD] = jnp.concatenate(pair, axis=0)
+    mine_at = pl.ds(pl.multiple_of(sp * mod_rows, 128), mod_rows)
+    act = act_ref[:, mine_at]
+    act_row = lax.broadcasted_iota(jnp.int32, act.shape, 0)
+    act = jnp.where(act_row < 2, act, 0.0).astype(bf16)
+    for which, name in enumerate(("shift", "scale")):
+        loads[name].wait()
+        got = jnp.dot(act, w_mod[which], preferred_element_type=f32)
+        part[2 * which : 2 * which + 2, :] = got[0:2, :]
+    pl.semaphore_wait(barrier, n_grp + n_sp + n_tp - 3)
+
+    def mod_copy(k):
+        return pltpu.make_async_remote_copy(
+            src_ref=part,
+            dst_ref=part_in.at[k - 1],
+            send_sem=mod_send.at[k - 1],
+            recv_sem=mod_recv.at[k - 1],
+            device_id={"sp": lax.rem(sp + k, n_sp)},
+            device_id_type=MESH,
+        )
+
+    for k in range(1, n_sp):
+        mod_copy(k).start()
+    load("gate", 2, w_gate_hbm, w_mod.at[2])
+    load("key", 5, w_key_hbm, w_key)
+    load("value", 6, w_value_hbm, w_value)
+    load("query", 7, w_query_hbm, w_query)
+    load("out", 8, w_out_hbm.at[:, pl.ds(0, shared)], w_all.at[tp])
+    load("rest", 9, w_out_hbm.at[:, pl.ds(shared, depth - shared)], w_rest)
+
+    def columns_of(group, i):
+        return pl.ds(pl.multiple_of((i * n_grp + group) * share, 128), share)
+
+    def source(k, which):
+        return lax.rem(chip - k + chips, chips) * 2 + which
+
+    def beside_own():
+        return pltpu.make_async_remote_copy(
+            src_ref=w_out_hbm.at[:, pl.ds(0, shared)],
+            dst_ref=w_all.at[tp],
+            send_sem=own_send.at[0],
+            recv_sem=own_recv.at[0],
+            device_id={"tp": partner},
+            device_id_type=MESH,
+        )
+
+    def across(k, i):
+        cols = columns_of(grp, i)
+        return pltpu.make_async_remote_copy(
+            src_ref=w_out_hbm.at[:, cols],
+            dst_ref=w_all.at[tp, :, cols],
+            send_sem=across_send.at[k - 1, i],
+            recv_sem=across_recv.at[k - 1, i],
+            device_id={"tp": lax.rem(chip + k, chips) * 2 + core},
+            device_id_type=MESH,
+        )
+
+    def relay(held, send, recv, to):
+        return pltpu.make_async_remote_copy(
+            src_ref=held,
+            dst_ref=held,
+            send_sem=send,
+            recv_sem=recv,
+            device_id=to,
+            device_id_type=MESH,
+        )
+
+    def beside(k, i, which=None):
+        which = core if which is None else which
+        held = w_all.at[source(k, which), :, columns_of(grp, i)]
+        return relay(
+            held, beside_send.at[k - 1, i], beside_recv.at[k - 1, i], {"tp": partner}
+        )
+
+    def over(j, k, i, group=None):
+        group = grp if group is None else group
+        held = w_all.at[source(k, core), :, columns_of(group, i)]
+        return relay(
+            held,
+            over_send.at[j - 1, k - 1, i],
+            over_recv.at[j - 1, k - 1, i],
+            {"grp": lax.rem(grp + j, n_grp)},
+        )
+
+    def last(j, k, i, which=None):
+        which = core if which is None else which
+        group = lax.rem(grp - j + n_grp, n_grp)
+        held = w_all.at[source(k, which), :, columns_of(group, i)]
+        return relay(
+            held,
+            last_send.at[j - 1, k - 1, i],
+            last_recv.at[j - 1, k - 1, i],
+            {"tp": partner},
+        )
+
+    def pass_on(i):
+        for k in range(1, chips):
+            across(k, i).wait_recv()
+            for j in range(1, n_grp):
+                over(j, k, i).start()
+            beside(k, i).start()
+
+    def pass_over(i):
+        for j in range(1, n_grp):
+            for k in range(1, chips):
+                over(j, k, i, lax.rem(grp - j + n_grp, n_grp)).wait_recv()
+                last(j, k, i).start()
+
+
     loads["latent"].wait()
     loads["context"].wait()
 
@@ -205,6 +327,10 @@
 
     for k in range(1, n_tp):
         mod2_copy(k).start()
+    beside_own().start()
+    for i in range(turns):
+        for k in range(1, chips):
+            across(k, i).start()
 
     def gate_copy(k):
         return pltpu.make_async_remote_copy(
@@ -310,8 +436,29 @@
             queries[at, cols] = turn(raw[:, cols], q_gain_ref[...], at).astype(bf16)
         return carry
 
+    stream = (n_sp - 1) * kv_chunks
+
+    def serve(j):
+        step = j // kv_chunks
+        c = lax.rem(j, kv_chunks)
+
+        @pl.when(jnp.logical_and(j < stream, jnp.logical_and(sp - 1 - step >= 0, sp < n_sp - 1)))
+        def _():
+            right_arrival(step, c).wait_recv()
+            right_copy(step + 1, c).start()
+
+        @pl.when(jnp.logical_and(j < stream, jnp.logical_and(sp + 1 + step <= n_sp - 1, sp > 0)))
+        def _():
+            left_arrival(step, c).wait_recv()
+            left_copy(step + 1, c).start()
+
     loads["query"].wait()
-    lax.fori_loop(0, tok // q_tile, project_queries, 0)
+    q_steps = tok // q_tile
+    for i in range(q_steps):
+        project_queries(i, 0)
+        if i == max(q_steps - 2, 0):
+            serve(jnp.int32(0))
+    serve(jnp.int32(1))
 
     scaling = HEAD ** (-0.5)
     a_tile = tile_of(tok, 128)
@@ -366,9 +513,15 @@
 
         lax.fori_loop(0, tok // a_tile, one, 0)
 
+    early = min(2, turns)
+    for i in range(early):
+        pass_on(i)
     attend(sp, 0, True)
+    serve(jnp.int32(2))
     for unit in range(1, units):
         attend(sp, unit, False)
+    serve(jnp.int32(3))
+    ahead = 4
 
     for k in range(1, n_sp):
         gate_copy(k).wait_recv()
@@ -379,42 +532,60 @@
     gate_mod[tp] = gate_whole
     for k in range(1, n_tp):
         gate2_copy(k).start()
+    if turns > early:
+        pass_on(early)
+
+    steps = (n_sp - 1) * units
+    events = {}
+    for i in range(early + 1, turns):
+        events.setdefault(min(2 * (i - early - 1), steps), []).append((pass_on, i))
+    for i in range(turns):
+        at = i if i < 4 else i + 1
+        if i == turns - 1:
+            at = steps
+        events.setdefault(min(at, steps), []).append((pass_over, i))
 
     def gather_step(t, carry):
         step = t // units
         unit = lax.rem(t, units)
         from_left = sp - 1 - step >= 0
         from_right = sp + 1 + step <= n_sp - 1
-        for k in range(per_unit):
-            c = unit * per_unit + k
-
-            @pl.when(from_left)
-            def _():
-                right_arrival(step, c).wait_recv()
-
-                @pl.when(sp < n_sp - 1)
-                def _():
-                    right_copy(step + 1, c).start()
-
-            @pl.when(from_right)
-            def _():
-                left_arrival(step, c).wait_recv()
-
-                @pl.when(sp > 0)
-                def _():
-                    left_copy(step + 1, c).start()
+        per = per_unit
+        for k in range((per + 1) // 2):
+            serve(ahead + t * per + k)
 
         @pl.when(from_left)
         def _():
+            @pl.when(sp == n_sp - 1)
+            def _():
+                for k in range(per):
+                    right_arrival(step, unit * per + k).wait_recv()
+
             attend(jnp.maximum(sp - 1 - step, 0), unit, False)
+
+        for k in range((per + 1) // 2, per):
+            serve(ahead + t * per + k)
 
         @pl.when(from_right)
         def _():
+            @pl.when(sp == 0)
+            def _():
+                for k in range(per):
+                    left_arrival(step, unit * per + k).wait_recv()
+
             attend(jnp.minimum(sp + 1 + step, n_sp - 1), unit, False)
 
+        for at in sorted(events):
+            if at < steps:
+
+                @pl.when(t == at)
+                def _():
+                    for act_on, i in events[at]:
+                        act_on(i)
+
         return carry
 
-    lax.fori_loop(0, (n_sp - 1) * units, gather_step, 0)
+    lax.fori_loop(0, steps, gather_step, 0)
 
     def finish(i, carry):
         at = pl.ds(pl.multiple_of(i * a_tile, 16), a_tile)
@@ -425,12 +596,24 @@
 
     lax.fori_loop(0, tok // a_tile, finish, 0)
 
-    chips = n_tp // 2
-    chip = tp // 2
-    core = lax.rem(tp, 2)
-    piece = tok // n_tp
+    def att_copy(k):
+        to = lax.rem(tp + k, n_tp)
+        return pltpu.make_async_remote_copy(
+            src_ref=attended.at[pl.ds(pl.multiple_of(to * piece, 16), piece)],
+            dst_ref=att_all.at[tp],
+            send_sem=att_send.at[k - 1],
+            recv_sem=att_recv.at[k - 1],
+            device_id={"tp": to},
+            device_id_type=MESH,
+        )
+
+    for k in range(1, n_tp):
+        att_copy(k).start()
+    att_all[tp] = attended[pl.ds(pl.multiple_of(tp * piece, 16), piece), :]
+    for act_on, i in events.get(steps, []):
+        act_on(i)
     width = pair_out.shape[3]
-    chunks = depth // width
+    chunks = pair_out.shape[1]
 
     def pair_copy(k, c):
         return pltpu.make_async_remote_copy(
@@ -438,7 +621,7 @@
             dst_ref=pair_in.at[k, c],
             send_sem=pair_send.at[k, c],
             recv_sem=pair_recv.at[k, c],
-            device_id={"tp": chip * 2 + 1 - core},
+            device_id={"tp": partner},
             device_id_type=MESH,
         )
 
@@ -459,7 +642,7 @@
         def part_of(which):
             at = pl.ds(pl.multiple_of((to * 2 + which) * piece, 16), piece)
             return jnp.dot(
-                attended[at, :], w_out[:, cols], preferred_element_type=f32
+                attended[at, :], w_rest[:, cols], preferred_element_type=f32
             ).astype(bf16)
 
         pair_out[k, c] = part_of(1 - core)
@@ -471,37 +654,69 @@
         far_out[k - 1, c] = (mine[k, c].astype(f32) + pair_in[k, c].astype(f32)).astype(bf16)
         far_copy(k, c).start()
 
+    loads["rest"].wait()
+    for k in range(1, chips):
+        for c in range(chunks):
+            multiply(k, c)
+        for c in range(chunks):
+            combine(k, c)
+    for c in range(chunks):
+        multiply(0, c)
+
+    def product(source_at, cols):
+        return (
+            jnp.dot(att_all[source_at], w_all[source_at, :, cols], preferred_element_type=f32)
+            .astype(bf16)
+            .astype(f32)
+        )
+
     loads["out"].wait()
-    for k in range(1, chips):
-        multiply(k, 0)
-
-        def far_step(c, carry):
-            multiply(k, c)
-            combine(k, c - 1)
-            return carry
-
-        lax.fori_loop(1, chunks, far_step, 0)
-        combine(k, chunks - 1)
-
-    def near_step(c, carry):
-        multiply(0, c)
-        return carry
-
-    lax.fori_loop(0, chunks, near_step, 0)
-
+    beside_own().wait_recv()
+    for k in range(1, n_tp):
+        att_copy(k).wait_recv()
+    blocks = shared // width
+    for c in range(blocks):
+        cols = slice(c * width, (c + 1) * width)
+        acc_out[:, cols] = product(tp, cols) + product(partner, cols)
+
+    for i in range(turns):
+        for k in range(1, chips):
+            beside(k, i, 1 - core).wait_recv()
+            for j in range(1, n_grp):
+                last(j, k, i, 1 - core).wait_recv()
     for k in range(1, n_tp):
         gate2_copy(k).wait_recv()
     per = mod_cols // width
+    for c in range(blocks):
+        cols = slice(c * width, (c + 1) * width)
+        result = acc_out[:, cols]
+        for k in range(1, chips):
+            for which in range(2):
+                result = result + product(source(k, which), cols)
+        first = (c % per) * width
+        gate = gate_mod[c // per, 0:1, first : first + width]
+        out_ref[:, cols] = (gate * result).astype(bf16)
     for c in range(chunks):
         pair_copy(0, c).wait_recv()
         result = mine[0, c].astype(f32) + pair_in[0, c].astype(f32)
         for k in range(1, chips):
             far_copy(k, c).wait_recv()
             result = result + far_in[k - 1, c].astype(f32)
-        first = (c % per) * width
-        gate = gate_mod[c // per, 0:1, first : first + width]
-        out_ref[:, c * width : (c + 1) * width] = (gate * result).astype(bf16)
-
+        at = blocks + c
+        first = (at % per) * width
+        gate = gate_mod[at // per, 0:1, first : first + width]
+        out_ref[:, at * width : (at + 1) * width] = (gate * result).astype(bf16)
+
+    beside_own().wait_send()
+    for k in range(1, n_tp):
+        att_copy(k).wait_send()
+    for k in range(1, chips):
+        for i in range(turns):
+            across(k, i).wait_send()
+            beside(k, i).wait_send()
+            for j in range(1, n_grp):
+                over(j, k, i).wait_send()
+                last(j, k, i).wait_send()
     for k in range(1, n_sp):
         mod_copy(k).wait_send()
         gate_copy(k).wait_send()
@@ -531,6 +746,7 @@
 
 
 def body(
+    n_grp,
     n_sp,
     n_tp,
     latent,
@@ -548,22 +764,19 @@
     k_gain,
     w_out,
 ):
-    sp = lax.axis_index("sp")
     tok, depth = latent.shape
     ctx = context.shape[0]
     rows = tok + ctx
     mod_rows, mod_cols = w_shift.shape
-    mine = [
-        lax.dynamic_slice_in_dim(cond, sp * mod_rows, mod_rows, 0)
-        for cond in (cond_latent, cond_context)
-    ]
-    row = lax.broadcasted_iota(jnp.int32, (16, mod_rows), 0)
-    act = jnp.where(row == 0, mine[0][None].astype(f32), mine[1][None].astype(f32))
-    act = jnp.where(row < 2, jax.nn.silu(act), 0.0).astype(bf16)
     chips = n_tp // 2
     piece = tok // n_tp
     width = min(512, mod_cols)
-    chunks = depth // width
+    share = min(256, width)
+    turns = (3 * depth // 4) // (n_grp * share)
+    shared = turns * n_grp * share
+    shared -= shared % width
+    turns = shared // (n_grp * share)
+    chunks = (depth - shared) // width
     kv_cols = w_key.shape[1]
     q_cols = w_query.shape[1]
     heads = q_cols // HEAD
@@ -571,19 +784,22 @@
     hbm = pl.BlockSpec(memory_space=pl.ANY)
     dma = pltpu.SemaphoreType.DMA
     far = max(chips - 1, 1)
+    others = max(n_grp - 1, 1)
     kv_chunks = rows // tile_of(rows, 128)
     return pl.pallas_call(
-        functools.partial(kernel, n_sp, n_tp, tok, ctx),
+        functools.partial(kernel, n_grp, n_sp, n_tp, tok, ctx, share),
         out_shape=jax.ShapeDtypeStruct((piece, depth), bf16),
-        in_specs=[vmem] * 4 + [hbm] * 9,
+        in_specs=[vmem] * 5 + [hbm] * 9,
         out_specs=vmem,
         scratch_shapes=[
+            pltpu.VMEM((16, depth), f32),
             pltpu.VMEM((rows, depth), bf16),
             pltpu.VMEM((3, mod_rows, mod_cols), bf16),
             pltpu.VMEM(w_query.shape, bf16),
             pltpu.VMEM(w_key.shape, bf16),
             pltpu.VMEM(w_value.shape, bf16),
-            pltpu.VMEM(w_out.shape, bf16),
+            pltpu.VMEM((n_tp, w_out.shape[0], shared), bf16),
+            pltpu.VMEM((w_out.shape[0], depth - shared), bf16),
             pltpu.VMEM((rows, 1), f32),
             pltpu.VMEM((rows, HEAD), f32),
             pltpu.VMEM((rows, HEAD), f32),
@@ -602,12 +818,14 @@
             pltpu.VMEM((heads, tok, 1), f32),
             pltpu.VMEM((tok, q_cols), f32),
             pltpu.VMEM((tok, q_cols), bf16),
+            pltpu.VMEM((n_tp, piece, q_cols), bf16),
+            pltpu.VMEM((piece, shared), f32),
             pltpu.VMEM((chips, chunks, piece, width), bf16),
             pltpu.VMEM((chips, chunks, piece, width), bf16),
             pltpu.VMEM((chips, chunks, piece, width), bf16),
             pltpu.VMEM((far, chunks, piece, width), bf16),
             pltpu.VMEM((far, chunks, piece, width), bf16),
-            dma((9,)),
+            dma((10,)),
             dma((n_sp - 1,)),
             dma((n_sp - 1,)),
             dma((n_tp - 1,)),
@@ -624,12 +842,25 @@
             dma((chips, chunks)),
             dma((far, chunks)),
             dma((far, chunks)),
+            dma((1,)),
+            dma((1,)),
+            dma((far, turns)),
+            dma((far, turns)),
+            dma((far, turns)),
+            dma((far, turns)),
+            dma((others, far, turns)),
+            dma((others, far, turns)),
+            dma((others, far, turns)),
+            dma((others, far, turns)),
+            dma((n_tp - 1,)),
+            dma((n_tp - 1,)),
         ],
         compiler_params=pltpu.CompilerParams(
             collective_id=0, has_side_effects=True, vmem_limit_bytes=60 * 1024 * 1024
         ),
     )(
-        act,
+        cond_latent.reshape(depth // HEAD, HEAD),
+        cond_context.reshape(depth // HEAD, HEAD),
         norm_gain.reshape(1, depth),
         q_gain.reshape(1, HEAD),
         k_gain.reshape(1, HEAD),
@@ -663,7 +894,7 @@
         P("tp", None),
     )
     return jax.shard_map(
-        functools.partial(body, mesh.shape["sp"], mesh.shape["tp"]),
+        functools.partial(body, mesh.shape["grp"], mesh.shape["sp"], mesh.shape["tp"]),
         mesh=mesh,
         in_specs=placed,
         out_specs=P(("grp", "sp", "tp"), None),

time: 75.5 us -> 69.7 us (0.923)
  Pallas kernels: 71.8 us -> 67.5 us
  other arithmetic: 1.42 us -> 0 us
    pallas_call x1, Pallas kernels: 71.8 us -> 67.5 us  [body(): pl.pallas_call(functools.partial(kernel, n_grp, n_sp, n_tp, tok, ctx, sha...]
    convert_element_type x2 -> x0, other arithmetic: 1.42 us -> none  [the longest x1 0.72 us: body(): act = jnp.where(row < 2, jax.nn.silu(act), 0.0).astype(bf16)]
where the time goes in v1:
time: 69.7 us; the launch traced here: 69.5 us
  Pallas kernels  67.5 us (97%)
  local copies, waits for them, and re-layouts  2.06 us (3%)
    pallas_call x1, Pallas kernels, body(): pl.pallas_call(functools.partial(kernel, n_grp, n_sp, n_tp, tok, ctx, sha...  67.5 us
    unnamed x1, local copies, waits for them, and re-layouts  2.06 us

profile of v1, /device:TPU:0, one launch (start us, length us, event | category | flops | bytes accessed | tf_op | source)
XLA Modules:
  0.0 69.5 jit_solution(2444117095007854354)
XLA Ops:
  0.0 67.5 %shard_map.136 = bf16[96,4096]{1,0:T(8,128)(2,1)} custom-call(bf16[32,128]{1,0:T(8,128)(2,1)} %bitcast.6, bf16[32,128]{1,0:T(8,128)(2,1)} %bitcast.7, f32[1,4096]{1,0:T(1,128)} %bitcast.5, f32[1,128]{1,0:T(1,128)} %bitcast.8, f32[1,128]{1,0:T(1,128)} %bitcast.9, bf16[384,4096]{1,0:T(8,128)(2,1)} %latent_hbm.1, bf16[64,4096]{1,0:T(8,128)(2,1)} %context_hbm.1, ...), custom_call_target="tpu_custom_call" | custom-call | tf_op jit(solution)/shard_map/pallas_call | solution.py:789
  67.5 2.1 %copy.16 = bf16[96,4096]{1,0:T(8,128)(2,1)} copy(bf16[96,4096]{1,0:T(8,128)(2,1)} %shard_map.136) | data formatting | bytes 1572864

commit v2 on v1

--- a/solution.py
+++ b/solution.py
@@ -38,11 +38,11 @@
     tok,
     ctx,
     share,
-    cond_latent_ref,
-    cond_context_ref,
-    gain_ref,
-    q_gain_ref,
-    k_gain_ref,
+    cond_latent_hbm,
+    cond_context_hbm,
+    gain_hbm,
+    q_gain_hbm,
+    k_gain_hbm,
     latent_hbm,
     context_hbm,
     w_shift_hbm,
@@ -52,6 +52,12 @@
     w_key_hbm,
     w_value_hbm,
     w_out_hbm,
+    out_hbm,
+    cond_latent_ref,
+    cond_context_ref,
+    gain_ref,
+    q_gain_ref,
+    k_gain_ref,
     out_ref,
     act_ref,
     x,
@@ -115,6 +121,7 @@
     last_recv,
     att_send,
     att_recv,
+    out_sem,
 ):
     grp = lax.axis_index("grp")
     sp = lax.axis_index("sp")
@@ -126,6 +133,7 @@
     piece = tok // n_tp
     turns = w_all.shape[2] // (n_grp * share)
     shared = w_all.shape[2]
+    mod_rows = w_mod.shape[1]
     rows = tok + ctx
     depth = x.shape[1]
     mod_cols = mod.shape[2]
@@ -144,10 +152,15 @@
         loads[name] = pltpu.make_async_copy(source, target, load_sem.at[index])
         loads[name].start()
 
+    load("cond_latent", 10, cond_latent_hbm, cond_latent_ref)
+    load("cond_context", 11, cond_context_hbm, cond_context_ref)
     load("shift", 0, w_shift_hbm, w_mod.at[0])
     load("scale", 1, w_scale_hbm, w_mod.at[1])
     load("latent", 3, latent_hbm, x.at[pl.ds(0, tok)])
     load("context", 4, context_hbm, x.at[pl.ds(tok, ctx)])
+    load("gain", 12, gain_hbm, gain_ref)
+    load("q_gain", 13, q_gain_hbm, q_gain_ref)
+    load("k_gain", 14, k_gain_hbm, k_gain_ref)
 
     barrier = pltpu.get_barrier_semaphore()
     for k in range(1, n_sp):
@@ -164,6 +177,197 @@
             barrier, inc=1, device_id={"grp": lax.rem(grp + k, n_grp)}, device_id_type=MESH
         )
 
+    loads["cond_latent"].wait()
+    loads["cond_context"].wait()
+    vectors = [ref[...].astype(f32) for ref in (cond_latent_ref, cond_context_ref)]
+    vectors = [vector * (1.0 / (1.0 + jnp.exp(-vector))) for vector in vectors]
+    lane_rows = depth // HEAD
+    for j in range(lane_rows):
+        pair = [vector[j : j + 1, :] for vector in vectors]
+        act_ref[0:2, j * HEAD : (j + 1) * HEAD] = jnp.concatenate(pair, axis=0)
+    mine_at = pl.ds(pl.multiple_of(sp * mod_rows, 128), mod_rows)
+    act = act_ref[:, mine_at]
+    act_row = lax.broadcasted_iota(jnp.int32, act.shape, 0)
+    act = jnp.where(act_row < 2, act, 0.0).astype(bf16)
+    for which, name in enumerate(("shift", "scale")):
+        loads[name].wait()
+        got = jnp.dot(act, w_mod[which], preferred_element_type=f32)
+        part[2 * which : 2 * which + 2, :] = got[0:2, :]
+    pl.semaphore_wait(barrier, n_grp + n_sp + n_tp - 3)
+
+    def all_of(held, send, recv):
+        return pltpu.make_async_remote_copy(
+            src_ref=held,
+            dst_ref=held,
+            send_sem=send,
+            recv_sem=recv,
+            device_id={"tp": partner},
+            device_id_type=MESH,
+        )
+
+    def mod_copy(k):
+        return pltpu.make_async_remote_copy(
+            src_ref=part,
+            dst_ref=part_in.at[k - 1],
+            send_sem=mod_send.at[0],
+            recv_sem=mod_recv.at[0],
+            device_id={"sp": lax.rem(sp + k, n_sp)},
+            device_id_type=MESH,
+        )
+
+    for k in range(1, n_sp):
+        mod_copy(k).start()
+    load("gate", 2, w_gate_hbm, w_mod.at[2])
+    load("key", 5, w_key_hbm, w_key)
+    load("value", 6, w_value_hbm, w_value)
+    load("query", 7, w_query_hbm, w_query)
+    load("out", 8, w_out_hbm.at[:, pl.ds(0, shared)], w_all.at[tp])
+    load("rest", 9, w_out_hbm.at[:, pl.ds(shared, depth - shared)], w_rest)
+
+    def columns_of(group, i):
+        return pl.ds(pl.multiple_of((i * n_grp + group) * share, 128), share)
+
+    def source(k, which):
+        return lax.rem(chip - k + chips, chips) * 2 + which
+
+    def beside_own():
+        return pltpu.make_async_remote_copy(
+            src_ref=w_out_hbm.at[:, pl.ds(0, shared)],
+            dst_ref=w_all.at[tp],
+            send_sem=own_send.at[0],
+            recv_sem=own_recv.at[0],
+            device_id={"tp": partner},
+            device_id_type=MESH,
+        )
+
+    def across(k, i):
+        cols = columns_of(grp, i)
+        return pltpu.make_async_remote_copy(
+            src_ref=w_out_hbm.at[:, cols],
+            dst_ref=w_all.at[tp, :, cols],
+            send_sem=across_send.at[0],
+            recv_sem=across_recv.at[k - 1, i],
+            device_id={"tp": lax.rem(chip + k, chips) * 2 + core},
+            device_id_type=MESH,
+        )
+
+    def relay(held, send, recv, to):
+        return pltpu.make_async_remote_copy(
+            src_ref=held,
+            dst_ref=held,
+            send_sem=send,
+            recv_sem=recv,
+            device_id=to,
+            device_id_type=MESH,
+        )
+
+    in_block = pair_out.shape[3] // (n_grp * share)
+    tail_from = turns - in_block
+
+    def batch_of(i):
+        return 0 if i < tail_from else 1
+
+    def beside(k, i, which=None):
+        which = core if which is None else which
+        held = w_all.at[source(k, which), :, columns_of(grp, i)]
+        return relay(
+            held, beside_send.at[0], beside_recv.at[batch_of(i)], {"tp": partner}
+        )
+
+    def over(j, k, i, group=None):
+        group = grp if group is None else group
+        held = w_all.at[source(k, core), :, columns_of(group, i)]
+        return relay(
+            held,
+            over_send.at[0],
+            over_recv.at[j - 1, k - 1, i],
+            {"grp": lax.rem(grp + j, n_grp)},
+        )
+
+    def last(j, k, i, which=None):
+        which = core if which is None else which
+        group = lax.rem(grp - j + n_grp, n_grp)
+        held = w_all.at[source(k, which), :, columns_of(group, i)]
+        return relay(
+            held,
+            last_send.at[0],
+            last_recv.at[batch_of(i)],
+            {"tp": partner},
+        )
+
+    def pass_on(i):
+        for k in range(1, chips):
+            across(k, i).wait_recv()
+            for j in range(1, n_grp):
+                over(j, k, i).start()
+            beside(k, i).start()
+
+    def pass_over(i):
+        for j in range(1, n_grp):
+            for k in range(1, chips):
+                over(j, k, i, lax.rem(grp - j + n_grp, n_grp)).wait_recv()
+                last(j, k, i).start()
+
+
+    loads["latent"].wait()
+    loads["context"].wait()
+
+    def stats(i, carry):
+        at = pl.ds(pl.multiple_of(i * 16, 16), 16)
+        piece = x[at, :].astype(f32)
+        inv[at, :] = lax.rsqrt(jnp.mean(piece * piece, axis=-1, keepdims=True) + epsilon)
+        return carry
+
+    lax.fori_loop(0, rows // 16, stats, 0, unroll=2)
+
+    all_of(part_in, mod_send.at[0], mod_recv.at[0]).wait_recv()
+    whole = part[...]
+    for k in range(1, n_sp):
+        whole = whole + part_in[k - 1]
+    summed[...] = whole
+    mod[tp] = whole
+
+    def mod2_copy(k):
+        return pltpu.make_async_remote_copy(
+            src_ref=summed,
+            dst_ref=mod.at[tp],
+            send_sem=mod2_send.at[0],
+            recv_sem=mod2_recv.at[0],
+            device_id={"tp": lax.rem(tp + k, n_tp)},
+            device_id_type=MESH,
+        )
+
+    for k in range(1, n_tp):
+        mod2_copy(k).start()
+    beside_own().start()
+    for i in range(turns):
+        for k in range(1, chips):
+            across(k, i).start()
+
+    def gate_copy(k):
+        return pltpu.make_async_remote_copy(
+            src_ref=gate_part,
+            dst_ref=gate_in.at[k - 1],
+            send_sem=gate_send.at[0],
+            recv_sem=gate_recv.at[0],
+            device_id={"sp": lax.rem(sp + k, n_sp)},
+            device_id_type=MESH,
+        )
+
+    def gate2_copy(k):
+        return pltpu.make_async_remote_copy(
+            src_ref=gate_sum,
+            dst_ref=gate_mod.at[tp],
+            send_sem=gate2_send.at[0],
+            recv_sem=gate2_recv.at[0],
+            device_id={"tp": lax.rem(tp + k, n_tp)},
+            device_id_type=MESH,
+        )
+
+    loads["gate"].wait()
+    gate_part[...] = jnp.dot(act, w_mod[2], preferred_element_type=f32)[0:2, :]
+    for k in range(1, n_sp):
+        gate_copy(k).start()
     def tables(i, carry):
         at = pl.ds(pl.multiple_of(i * 16, 16), 16)
         index = i * 16 + lax.broadcasted_iota(jnp.int32, (16, HEAD), 0)
@@ -181,183 +385,9 @@
         return carry
 
     lax.fori_loop(0, rows // 16, tables, 0)
-    mod_rows = w_mod.shape[1]
-    vectors = [ref[...].astype(f32) for ref in (cond_latent_ref, cond_context_ref)]
-    vectors = [vector * (1.0 / (1.0 + jnp.exp(-vector))) for vector in vectors]
-    lane_rows = depth // HEAD
-    for j in range(lane_rows):
-        pair = [vector[j : j + 1, :] for vector in vectors]
-        act_ref[0:2, j * HEAD : (j + 1) * HEAD] = jnp.concatenate(pair, axis=0)
-    mine_at = pl.ds(pl.multiple_of(sp * mod_rows, 128), mod_rows)
-    act = act_ref[:, mine_at]
-    act_row = lax.broadcasted_iota(jnp.int32, act.shape, 0)
-    act = jnp.where(act_row < 2, act, 0.0).astype(bf16)
-    for which, name in enumerate(("shift", "scale")):
+    all_of(mod.at[pl.ds(0, n_tp - 1)], mod2_send.at[0], mod2_recv.at[0]).wait_recv()
+    for name in ("gain", "q_gain", "k_gain"):
         loads[name].wait()
-        got = jnp.dot(act, w_mod[which], preferred_element_type=f32)
-        part[2 * which : 2 * which + 2, :] = got[0:2, :]
-    pl.semaphore_wait(barrier, n_grp + n_sp + n_tp - 3)
-
-    def mod_copy(k):
-        return pltpu.make_async_remote_copy(
-            src_ref=part,
-            dst_ref=part_in.at[k - 1],
-            send_sem=mod_send.at[k - 1],
-            recv_sem=mod_recv.at[k - 1],
-            device_id={"sp": lax.rem(sp + k, n_sp)},
-            device_id_type=MESH,
-        )
-
-    for k in range(1, n_sp):
-        mod_copy(k).start()
-    load("gate", 2, w_gate_hbm, w_mod.at[2])
-    load("key", 5, w_key_hbm, w_key)
-    load("value", 6, w_value_hbm, w_value)
-    load("query", 7, w_query_hbm, w_query)
-    load("out", 8, w_out_hbm.at[:, pl.ds(0, shared)], w_all.at[tp])
-    load("rest", 9, w_out_hbm.at[:, pl.ds(shared, depth - shared)], w_rest)
-
-    def columns_of(group, i):
-        return pl.ds(pl.multiple_of((i * n_grp + group) * share, 128), share)
-
-    def source(k, which):
-        return lax.rem(chip - k + chips, chips) * 2 + which
-
-    def beside_own():
-        return pltpu.make_async_remote_copy(
-            src_ref=w_out_hbm.at[:, pl.ds(0, shared)],
-            dst_ref=w_all.at[tp],
-            send_sem=own_send.at[0],
-            recv_sem=own_recv.at[0],
-            device_id={"tp": partner},
-            device_id_type=MESH,
-        )
-
-    def across(k, i):
-        cols = columns_of(grp, i)
-        return pltpu.make_async_remote_copy(
-            src_ref=w_out_hbm.at[:, cols],
-            dst_ref=w_all.at[tp, :, cols],
-            send_sem=across_send.at[k - 1, i],
-            recv_sem=across_recv.at[k - 1, i],
-            device_id={"tp": lax.rem(chip + k, chips) * 2 + core},
-            device_id_type=MESH,
-        )
-
-    def relay(held, send, recv, to):
-        return pltpu.make_async_remote_copy(
-            src_ref=held,
-            dst_ref=held,
-            send_sem=send,
-            recv_sem=recv,
-            device_id=to,
-            device_id_type=MESH,
-        )
-
-    def beside(k, i, which=None):
-        which = core if which is None else which
-        held = w_all.at[source(k, which), :, columns_of(grp, i)]
-        return relay(
-            held, beside_send.at[k - 1, i], beside_recv.at[k - 1, i], {"tp": partner}
-        )
-
-    def over(j, k, i, group=None):
-        group = grp if group is None else group
-        held = w_all.at[source(k, core), :, columns_of(group, i)]
-        return relay(
-            held,
-            over_send.at[j - 1, k - 1, i],
-            over_recv.at[j - 1, k - 1, i],
-            {"grp": lax.rem(grp + j, n_grp)},
-        )
-
-    def last(j, k, i, which=None):
-        which = core if which is None else which
-        group = lax.rem(grp - j + n_grp, n_grp)
-        held = w_all.at[source(k, which), :, columns_of(group, i)]
-        return relay(
-            held,
-            last_send.at[j - 1, k - 1, i],
-            last_recv.at[j - 1, k - 1, i],
-            {"tp": partner},
-        )
-
-    def pass_on(i):
-        for k in range(1, chips):
-            across(k, i).wait_recv()
-            for j in range(1, n_grp):
-                over(j, k, i).start()
-            beside(k, i).start()
-
-    def pass_over(i):
-        for j in range(1, n_grp):
-            for k in range(1, chips):
-                over(j, k, i, lax.rem(grp - j + n_grp, n_grp)).wait_recv()
-                last(j, k, i).start()
-
-
-    loads["latent"].wait()
-    loads["context"].wait()
-
-    def stats(i, carry):
-        at = pl.ds(pl.multiple_of(i * 16, 16), 16)
-        piece = x[at, :].astype(f32)
-        inv[at, :] = lax.rsqrt(jnp.mean(piece * piece, axis=-1, keepdims=True) + epsilon)
-        return carry
-
-    lax.fori_loop(0, rows // 16, stats, 0, unroll=2)
-
-    for k in range(1, n_sp):
-        mod_copy(k).wait_recv()
-    whole = part[...]
-    for k in range(1, n_sp):
-        whole = whole + part_in[k - 1]
-    summed[...] = whole
-    mod[tp] = whole
-
-    def mod2_copy(k):
-        return pltpu.make_async_remote_copy(
-            src_ref=summed,
-            dst_ref=mod.at[tp],
-            send_sem=mod2_send.at[k - 1],
-            recv_sem=mod2_recv.at[k - 1],
-            device_id={"tp": lax.rem(tp + k, n_tp)},
-            device_id_type=MESH,
-        )
-
-    for k in range(1, n_tp):
-        mod2_copy(k).start()
-    beside_own().start()
-    for i in range(turns):
-        for k in range(1, chips):
-            across(k, i).start()
-
-    def gate_copy(k):
-        return pltpu.make_async_remote_copy(
-            src_ref=gate_part,
-            dst_ref=gate_in.at[k - 1],
-            send_sem=gate_send.at[k - 1],
-            recv_sem=gate_recv.at[k - 1],
-            device_id={"sp": lax.rem(sp + k, n_sp)},
-            device_id_type=MESH,
-        )
-
-    def gate2_copy(k):
-        return pltpu.make_async_remote_copy(
-            src_ref=gate_sum,
-            dst_ref=gate_mod.at[tp],
-            send_sem=gate2_send.at[k - 1],
-            recv_sem=gate2_recv.at[k - 1],
-            device_id={"tp": lax.rem(tp + k, n_tp)},
-            device_id_type=MESH,
-        )
-
-    loads["gate"].wait()
-    gate_part[...] = jnp.dot(act, w_mod[2], preferred_element_type=f32)[0:2, :]
-    for k in range(1, n_sp):
-        gate_copy(k).start()
-    for k in range(1, n_tp):
-        mod2_copy(k).wait_recv()
 
     def normalize(low, high):
         for start in range(low, high, 16):
@@ -381,7 +411,7 @@
         return pltpu.make_async_remote_copy(
             src_ref=held,
             dst_ref=held,
-            send_sem=send.at[step, c],
+            send_sem=send.at[0],
             recv_sem=recv.at[step, c],
             device_id={"sp": to},
             device_id_type=MESH,
@@ -403,6 +433,10 @@
         return stream_copy(
             jnp.minimum(sp + 1 + step, n_sp - 1), step, c, left_send, left_recv, to_left
         )
+
+    def early_pass(act_on, i):
+        if i < turns:
+            act_on(i)
 
     for c in range(kv_chunks):
         low, high = c * kv_tile, (c + 1) * kv_tile
@@ -426,6 +460,10 @@
         def _():
             left_copy(0, c).start()
 
+        if c == min(1, kv_chunks - 1):
+            early_pass(pass_on, 0)
+
+    early_pass(pass_on, 1)
     q_tile = tile_of(tok, 256)
 
     def project_queries(i, carry):
@@ -513,18 +551,18 @@
 
         lax.fori_loop(0, tok // a_tile, one, 0)
 
-    early = min(2, turns)
-    for i in range(early):
-        pass_on(i)
+    early_pass(pass_on, 2)
     attend(sp, 0, True)
+    early_pass(pass_over, 0)
     serve(jnp.int32(2))
     for unit in range(1, units):
         attend(sp, unit, False)
     serve(jnp.int32(3))
     ahead = 4
-
-    for k in range(1, n_sp):
-        gate_copy(k).wait_recv()
+    early_pass(pass_on, 3)
+    early_pass(pass_over, 1)
+
+    all_of(gate_in, gate_send.at[0], gate_recv.at[0]).wait_recv()
     gate_whole = gate_part[...]
     for k in range(1, n_sp):
         gate_whole = gate_whole + gate_in[k - 1]
@@ -532,18 +570,24 @@
     gate_mod[tp] = gate_whole
     for k in range(1, n_tp):
         gate2_copy(k).start()
-    if turns > early:
-        pass_on(early)
-
     steps = (n_sp - 1) * units
     events = {}
-    for i in range(early + 1, turns):
-        events.setdefault(min(2 * (i - early - 1), steps), []).append((pass_on, i))
-    for i in range(turns):
-        at = i if i < 4 else i + 1
-        if i == turns - 1:
-            at = steps
-        events.setdefault(min(at, steps), []).append((pass_over, i))
+    halves = 2 * steps
+    for i in range(4, turns):
+        at = (0, 1, 2, 3, 5, 7, 9, 11)[i - 4] if i < 12 else i
+        events.setdefault(min(at, halves - 1), []).append((pass_on, i))
+    for i in range(2, turns):
+        at = (1, 3, 4, 5, 6, 8, 10)[i - 2] if i < 9 else halves
+        events.setdefault(min(at, halves), []).append((pass_over, i))
+
+    def take_events(t, half):
+        for at in sorted(events):
+            if at < halves and at % 2 == half:
+
+                @pl.when(t == at // 2)
+                def _():
+                    for act_on, i in events[at]:
+                        act_on(i)
 
     def gather_step(t, carry):
         step = t // units
@@ -566,6 +610,8 @@
         for k in range((per + 1) // 2, per):
             serve(ahead + t * per + k)
 
+        take_events(t, 0)
+
         @pl.when(from_right)
         def _():
             @pl.when(sp == 0)
@@ -575,43 +621,34 @@
 
             attend(jnp.minimum(sp + 1 + step, n_sp - 1), unit, False)
 
-        for at in sorted(events):
-            if at < steps:
-
-                @pl.when(t == at)
-                def _():
-                    for act_on, i in events[at]:
-                        act_on(i)
-
+        take_events(t, 1)
         return carry
 
     lax.fori_loop(0, steps, gather_step, 0)
 
-    def finish(i, carry):
-        at = pl.ds(pl.multiple_of(i * a_tile, 16), a_tile)
+    def att_copy(k):
+        to = lax.rem(tp + k, n_tp)
+        return pltpu.make_async_remote_copy(
+            src_ref=attended.at[pl.ds(pl.multiple_of(to * piece, 16), piece)],
+            dst_ref=att_all.at[tp],
+            send_sem=att_send.at[0],
+            recv_sem=att_recv.at[jnp.where(to == partner, 0, 1)],
+            device_id={"tp": to},
+            device_id_type=MESH,
+        )
+
+    def finish(k):
+        at = pl.ds(pl.multiple_of(lax.rem(tp + k, n_tp) * piece, 16), piece)
         for h in range(heads):
             cols = slice(h * HEAD, (h + 1) * HEAD)
             attended[at, cols] = (acc[at, cols] / total[h, at, :]).astype(bf16)
-        return carry
-
-    lax.fori_loop(0, tok // a_tile, finish, 0)
-
-    def att_copy(k):
-        to = lax.rem(tp + k, n_tp)
-        return pltpu.make_async_remote_copy(
-            src_ref=attended.at[pl.ds(pl.multiple_of(to * piece, 16), piece)],
-            dst_ref=att_all.at[tp],
-            send_sem=att_send.at[k - 1],
-            recv_sem=att_recv.at[k - 1],
-            device_id={"tp": to},
-            device_id_type=MESH,
-        )
-
-    for k in range(1, n_tp):
-        att_copy(k).start()
+
+    for k in range(2, n_tp + 2):
+        finish(k)
+        if k % n_tp:
+            att_copy(k % n_tp).start()
     att_all[tp] = attended[pl.ds(pl.multiple_of(tp * piece, 16), piece), :]
-    for act_on, i in events.get(steps, []):
-        act_on(i)
+    late = events.get(halves, [])
     width = pair_out.shape[3]
     chunks = pair_out.shape[1]
 
@@ -619,7 +656,7 @@
         return pltpu.make_async_remote_copy(
             src_ref=pair_out.at[k, c],
             dst_ref=pair_in.at[k, c],
-            send_sem=pair_send.at[k, c],
+            send_sem=pair_send.at[0],
             recv_sem=pair_recv.at[k, c],
             device_id={"tp": partner},
             device_id_type=MESH,
@@ -629,7 +666,7 @@
         return pltpu.make_async_remote_copy(
             src_ref=far_out.at[k - 1, c],
             dst_ref=far_in.at[k - 1, c],
-            send_sem=far_send.at[k - 1, c],
+            send_sem=far_send.at[0],
             recv_sem=far_recv.at[k - 1, c],
             device_id={"tp": lax.rem(chip + k, chips) * 2 + core},
             device_id_type=MESH,
@@ -654,14 +691,7 @@
         far_out[k - 1, c] = (mine[k, c].astype(f32) + pair_in[k, c].astype(f32)).astype(bf16)
         far_copy(k, c).start()
 
-    loads["rest"].wait()
-    for k in range(1, chips):
-        for c in range(chunks):
-            multiply(k, c)
-        for c in range(chunks):
-            combine(k, c)
-    for c in range(chunks):
-        multiply(0, c)
+    blocks = shared // width
 
     def product(source_at, cols):
         return (
@@ -670,79 +700,94 @@
             .astype(f32)
         )
 
+    loads["rest"].wait()
     loads["out"].wait()
-    beside_own().wait_recv()
-    for k in range(1, n_tp):
-        att_copy(k).wait_recv()
-    blocks = shared // width
+    for k in range(1, chips):
+        for c in range(chunks):
+            multiply(k, c)
     for c in range(blocks):
         cols = slice(c * width, (c + 1) * width)
-        acc_out[:, cols] = product(tp, cols) + product(partner, cols)
-
-    for i in range(turns):
-        for k in range(1, chips):
-            beside(k, i, 1 - core).wait_recv()
-            for j in range(1, n_grp):
-                last(j, k, i, 1 - core).wait_recv()
-    for k in range(1, n_tp):
-        gate2_copy(k).wait_recv()
+        acc_out[:, cols] = product(tp, cols)
+    for k in range(1, chips):
+        for c in range(chunks):
+            combine(k, c)
+    for c in range(chunks):
+        multiply(0, c)
+    beside_own().wait_recv()
+    all_of(att_all.at[pl.ds(0, 1)], att_send.at[0], att_recv.at[0]).wait_recv()
+    for c in range(blocks):
+        cols = slice(c * width, (c + 1) * width)
+        acc_out[:, cols] += product(partner, cols)
+    for act_on, i in late:
+        act_on(i)
+    if chips > 1:
+        all_of(att_all.at[pl.ds(0, n_tp - 2)], att_send.at[0], att_recv.at[1]).wait_recv()
+
+    all_of(gate_mod.at[pl.ds(0, n_tp - 1)], gate2_send.at[0], gate2_recv.at[0]).wait_recv()
     per = mod_cols // width
+
+    def put(at, result):
+        cols = slice(at * width, (at + 1) * width)
+        first = (at % per) * width
+        gate = gate_mod[at // per, 0:1, first : first + width]
+        out_ref[:, cols] = (gate * result).astype(bf16)
+        out_copy(at).start()
+
+    def out_copy(at):
+        cols = pl.ds(at * width, width)
+        return pltpu.make_async_copy(out_ref.at[:, cols], out_hbm.at[:, cols], out_sem.at[0])
+
     for c in range(blocks):
+        if chips > 1 and c in (0, blocks - 1):
+            batch = 0 if c == 0 and blocks > 1 else 1
+            count = (tail_from if batch == 0 else in_block) * share
+            for copies, sems in ((1, beside_recv), (n_grp - 1, last_recv)):
+                if copies * count:
+                    held = w_all.at[pl.ds(0, chips - 1), :, pl.ds(0, copies * count)]
+                    all_of(held, own_send.at[0], sems.at[batch]).wait_recv()
         cols = slice(c * width, (c + 1) * width)
         result = acc_out[:, cols]
         for k in range(1, chips):
             for which in range(2):
                 result = result + product(source(k, which), cols)
-        first = (c % per) * width
-        gate = gate_mod[c // per, 0:1, first : first + width]
-        out_ref[:, cols] = (gate * result).astype(bf16)
+        put(c, result)
     for c in range(chunks):
         pair_copy(0, c).wait_recv()
         result = mine[0, c].astype(f32) + pair_in[0, c].astype(f32)
         for k in range(1, chips):
             far_copy(k, c).wait_recv()
             result = result + far_in[k - 1, c].astype(f32)
-        at = blocks + c
-        first = (at % per) * width
-        gate = gate_mod[at // per, 0:1, first : first + width]
-        out_ref[:, at * width : (at + 1) * width] = (gate * result).astype(bf16)
+        put(blocks + c, result)
 
     beside_own().wait_send()
-    for k in range(1, n_tp):
-        att_copy(k).wait_send()
-    for k in range(1, chips):
-        for i in range(turns):
-            across(k, i).wait_send()
-            beside(k, i).wait_send()
-            for j in range(1, n_grp):
-                over(j, k, i).wait_send()
-                last(j, k, i).wait_send()
-    for k in range(1, n_sp):
-        mod_copy(k).wait_send()
-        gate_copy(k).wait_send()
-    for k in range(1, n_tp):
-        mod2_copy(k).wait_send()
-        gate2_copy(k).wait_send()
-
-    def drain(step, carry):
-        for which in range(kv_chunks):
-
-            @pl.when(jnp.logical_and(sp < n_sp - 1, sp - step >= 0))
-            def _():
-                right_copy(step, which).wait_send()
-
-            @pl.when(jnp.logical_and(sp > 0, sp + step <= n_sp - 1))
-            def _():
-                left_copy(step, which).wait_send()
-
-        return carry
-
-    lax.fori_loop(0, n_sp - 1, drain, 0)
-    for c in range(chunks):
-        pair_copy(0, c).wait_send()
-        for k in range(1, chips):
-            pair_copy(k, c).wait_send()
-            far_copy(k, c).wait_send()
+    all_of(att_all.at[pl.ds(0, n_tp - 1)], att_send.at[0], att_recv.at[0]).wait_send()
+    if chips > 1:
+        count = turns * share
+        held = w_all.at[pl.ds(0, chips - 1), :, pl.ds(0, count)]
+        all_of(held, across_send.at[0], own_recv.at[0]).wait_send()
+        all_of(held, beside_send.at[0], own_recv.at[0]).wait_send()
+        if n_grp > 1:
+            held = w_all.at[pl.ds(0, chips - 1), :, pl.ds(0, (n_grp - 1) * count)]
+            all_of(held, over_send.at[0], own_recv.at[0]).wait_send()
+            all_of(held, last_send.at[0], own_recv.at[0]).wait_send()
+    all_of(part_in, mod_send.at[0], mod_recv.at[0]).wait_send()
+    all_of(gate_in, gate_send.at[0], gate_recv.at[0]).wait_send()
+    all_of(mod.at[pl.ds(0, n_tp - 1)], mod2_send.at[0], mod2_recv.at[0]).wait_send()
+    all_of(gate_mod.at[pl.ds(0, n_tp - 1)], gate2_send.at[0], gate2_recv.at[0]).wait_send()
+
+    for at in range(n_sp):
+
+        @pl.when(sp == at)
+        def _():
+            if at < n_sp - 1:
+                all_of(kv.at[pl.ds(0, at + 1)], right_send.at[0], right_recv.at[0, 0]).wait_send()
+            if at > 0:
+                all_of(kv.at[pl.ds(0, n_sp - at)], left_send.at[0], left_recv.at[0, 0]).wait_send()
+
+    all_of(pair_out, pair_send.at[0], pair_recv.at[0, 0]).wait_send()
+    if chips > 1:
+        all_of(far_out, far_send.at[0], far_recv.at[0, 0]).wait_send()
+    pltpu.make_async_copy(out_ref, out_hbm, out_sem.at[0]).wait()
 
 
 def body(
@@ -771,7 +816,7 @@
     chips = n_tp // 2
     piece = tok // n_tp
     width = min(512, mod_cols)
-    share = min(256, width)
+    share = min(128, width)
     turns = (3 * depth // 4) // (n_grp * share)
     shared = turns * n_grp * share
     shared -= shared % width
@@ -780,7 +825,6 @@
     kv_cols = w_key.shape[1]
     q_cols = w_query.shape[1]
     heads = q_cols // HEAD
-    vmem = pl.BlockSpec(memory_space=pltpu.VMEM)
     hbm = pl.BlockSpec(memory_space=pl.ANY)
     dma = pltpu.SemaphoreType.DMA
     far = max(chips - 1, 1)
@@ -789,9 +833,15 @@
     return pl.pallas_call(
         functools.partial(kernel, n_grp, n_sp, n_tp, tok, ctx, share),
         out_shape=jax.ShapeDtypeStruct((piece, depth), bf16),
-        in_specs=[vmem] * 5 + [hbm] * 9,
-        out_specs=vmem,
+        in_specs=[hbm] * 14,
+        out_specs=hbm,
         scratch_shapes=[
+            pltpu.VMEM((depth // HEAD, HEAD), bf16),
+            pltpu.VMEM((depth // HEAD, HEAD), bf16),
+            pltpu.VMEM((1, depth), f32),
+            pltpu.VMEM((1, HEAD), f32),
+            pltpu.VMEM((1, HEAD), f32),
+            pltpu.VMEM((piece, depth), bf16),
             pltpu.VMEM((16, depth), f32),
             pltpu.VMEM((rows, depth), bf16),
             pltpu.VMEM((3, mod_rows, mod_cols), bf16),
@@ -825,35 +875,36 @@
             pltpu.VMEM((chips, chunks, piece, width), bf16),
             pltpu.VMEM((far, chunks, piece, width), bf16),
             pltpu.VMEM((far, chunks, piece, width), bf16),
-            dma((10,)),
-            dma((n_sp - 1,)),
-            dma((n_sp - 1,)),
-            dma((n_tp - 1,)),
-            dma((n_tp - 1,)),
-            dma((n_sp - 1,)),
-            dma((n_sp - 1,)),
-            dma((n_tp - 1,)),
-            dma((n_tp - 1,)),
-            dma((n_sp, kv_chunks)),
-            dma((n_sp, kv_chunks)),
-            dma((n_sp, kv_chunks)),
-            dma((n_sp, kv_chunks)),
+            dma((15,)),
+            dma((1,)),
+            dma((1,)),
+            dma((1,)),
+            dma((1,)),
+            dma((1,)),
+            dma((1,)),
+            dma((1,)),
+            dma((1,)),
+            dma((1,)),
+            dma((n_sp - 1, kv_chunks)),
+            dma((1,)),
+            dma((n_sp - 1, kv_chunks)),
+            dma((1,)),
             dma((chips, chunks)),
-            dma((chips, chunks)),
+            dma((1,)),
             dma((far, chunks)),
-            dma((far, chunks)),
+            dma((1,)),
             dma((1,)),
             dma((1,)),
             dma((far, turns)),
-            dma((far, turns)),
-            dma((far, turns)),
-            dma((far, turns)),
+            dma((1,)),
+            dma((2,)),
+            dma((1,)),
             dma((others, far, turns)),
-            dma((others, far, turns)),
-            dma((others, far, turns)),
-            dma((others, far, turns)),
-            dma((n_tp - 1,)),
-            dma((n_tp - 1,)),
+            dma((1,)),
+            dma((2,)),
+            dma((1,)),
+            dma((2,)),
+            dma((1,)),
         ],
         compiler_params=pltpu.CompilerParams(
             collective_id=0, has_side_effects=True, vmem_limit_bytes=60 * 1024 * 1024

time: 69.7 us -> 61.5 us (0.88)
  Pallas kernels: 67.5 us -> 59.3 us
    pallas_call x1, Pallas kernels: 67.5 us -> 59.3 us  [body(): pl.pallas_call(functools.partial(kernel, n_grp, n_sp, n_tp, tok, ctx, sha...]
where the time goes in v2:
time: 61.5 us; the launch traced here: 61.3 us
  Pallas kernels  59.3 us (96%)
  local copies, waits for them, and re-layouts  2.06 us (3%)
    pallas_call x1, Pallas kernels, body(): pl.pallas_call(functools.partial(kernel, n_grp, n_sp, n_tp, tok, ctx, sha...  59.3 us
    unnamed x1, local copies, waits for them, and re-layouts  2.06 us

profile of v2, /device:TPU:0, one launch (start us, length us, event | category | flops | bytes accessed | tf_op | source)
XLA Modules:
  0.0 61.3 jit_solution(4361102845454374149)
XLA Ops:
  0.0 59.3 %shard_map.136 = bf16[96,4096]{1,0:T(8,128)(2,1)} custom-call(bf16[32,128]{1,0:T(8,128)(2,1)} %bitcast.6, bf16[32,128]{1,0:T(8,128)(2,1)} %bitcast.7, f32[1,4096]{1,0:T(1,128)} %bitcast.5, f32[1,128]{1,0:T(1,128)} %bitcast.8, f32[1,128]{1,0:T(1,128)} %bitcast.9, bf16[384,4096]{1,0:T(8,128)(2,1)} %latent_hbm.1, bf16[64,4096]{1,0:T(8,128)(2,1)} %context_hbm.1, ...), custom_call_target="tpu_custom_call" | custom-call | tf_op jit(solution)/shard_map/pallas_call | solution.py:833
  59.3 2.1 %copy.16 = bf16[96,4096]{1,0:T(8,128)(2,1)} copy(bf16[96,4096]{1,0:T(8,128)(2,1)} %shard_map.136) | data formatting | bytes 1572864

commit v3 on v2

--- a/solution.py
+++ b/solution.py
@@ -390,15 +390,16 @@
         loads[name].wait()
 
     def normalize(low, high):
-        for start in range(low, high, 16):
-            row = 0 if start < tok else 1
-            at = slice(start, start + 16)
-            for j in range(n_tp):
-                cols = slice(j * mod_cols, (j + 1) * mod_cols)
-                factor = gain_ref[:, cols] * (1.0 + mod[j, 2 + row : 3 + row, :])
-                shift = mod[j, row : row + 1, :]
-                piece = x[at, cols].astype(f32)
-                x[at, cols] = (piece * inv[at, :] * factor + shift).astype(bf16)
+        for j in range(n_tp):
+            cols = slice(j * mod_cols, (j + 1) * mod_cols)
+            for row, first, end in ((0, low, min(high, tok)), (1, max(low, tok), high)):
+                if first < end:
+                    factor = gain_ref[:, cols] * (1.0 + mod[j, 2 + row : 3 + row, :])
+                    shift = mod[j, row : row + 1, :]
+                    for start in range(first, end, 16):
+                        at = slice(start, start + 16)
+                        piece = x[at, cols].astype(f32)
+                        x[at, cols] = (piece * inv[at, :] * factor + shift).astype(bf16)
 
     def turn(vector, gain, at):
         vector = vector * lax.rsqrt(jnp.mean(vector * vector, axis=-1, keepdims=True) + epsilon) * gain
@@ -501,9 +502,10 @@
     scaling = HEAD ** (-0.5)
     a_tile = tile_of(tok, 128)
 
-    def attend(block, unit, first):
-        held = pl.ds(pl.multiple_of(unit * unit_rows, 16), unit_rows)
-        lane = unit * unit_rows + lax.broadcasted_iota(jnp.int32, (1, unit_rows), 1)
+    def attend(block, unit, first, size=None):
+        size = unit_rows if size is None else size
+        held = pl.ds(pl.multiple_of(unit * size, 16), size)
+        lane = unit * size + lax.broadcasted_iota(jnp.int32, (1, size), 1)
         lift = jnp.where(lane >= tok, context_lift, 0.0).astype(f32)
         spans = [slice(h * HEAD, (h + 1) * HEAD) for h in range(heads)]
 
@@ -549,7 +551,7 @@
                 acc[at, spans[h]] = products[h]
             return carry
 
-        lax.fori_loop(0, tok // a_tile, one, 0)
+        lax.fori_loop(0, tok // a_tile, one, 0, unroll=True)
 
     early_pass(pass_on, 2)
     attend(sp, 0, True)
@@ -624,7 +626,22 @@
         take_events(t, 1)
         return carry
 
-    lax.fori_loop(0, steps, gather_step, 0)
+    lax.fori_loop(0, steps - 1, gather_step, 0)
+    take_events(jnp.int32(steps - 1), 0)
+    for k in range(per_unit):
+        c = (units - 1) * per_unit + k
+
+        @pl.when(sp == n_sp - 1)
+        def _():
+            right_arrival(n_sp - 2, c).wait_recv()
+            attend(0, c, False, kv_tile)
+
+        @pl.when(sp == 0)
+        def _():
+            left_arrival(n_sp - 2, c).wait_recv()
+            attend(n_sp - 1, c, False, kv_tile)
+
+    take_events(jnp.int32(steps - 1), 1)
 
     def att_copy(k):
         to = lax.rem(tp + k, n_tp)

time: 61.5 us -> 60.8 us (0.989)
  Pallas kernels: 59.3 us -> 58.5 us
    pallas_call x1, Pallas kernels: 59.3 us -> 58.5 us  [body(): pl.pallas_call(functools.partial(kernel, n_grp, n_sp, n_tp, tok, ctx, sha...]
where the time goes in v3:
time: 60.8 us; the launch traced here: 60.6 us
  Pallas kernels  58.5 us (96%)
  local copies, waits for them, and re-layouts  2.06 us (3%)
    pallas_call x1, Pallas kernels, body(): pl.pallas_call(functools.partial(kernel, n_grp, n_sp, n_tp, tok, ctx, sha...  58.5 us
    unnamed x1, local copies, waits for them, and re-layouts  2.06 us

profile of v3, /device:TPU:0, one launch (start us, length us, event | category | flops | bytes accessed | tf_op | source)
XLA Modules:
  0.0 60.6 jit_solution(16450957683618604097)
XLA Ops:
  0.0 58.5 %shard_map.136 = bf16[96,4096]{1,0:T(8,128)(2,1)} custom-call(bf16[32,128]{1,0:T(8,128)(2,1)} %bitcast.6, bf16[32,128]{1,0:T(8,128)(2,1)} %bitcast.7, f32[1,4096]{1,0:T(1,128)} %bitcast.5, f32[1,128]{1,0:T(1,128)} %bitcast.8, f32[1,128]{1,0:T(1,128)} %bitcast.9, bf16[384,4096]{1,0:T(8,128)(2,1)} %latent_hbm.1, bf16[64,4096]{1,0:T(8,128)(2,1)} %context_hbm.1, ...), custom_call_target="tpu_custom_call" | custom-call | tf_op jit(solution)/shard_map/pallas_call | solution.py:850
  58.5 2.1 %copy.16 = bf16[96,4096]{1,0:T(8,128)(2,1)} copy(bf16[96,4096]{1,0:T(8,128)(2,1)} %shard_map.136) | data formatting | bytes 1572864
